TPU v7x, 32 devices: a whole 2x2x4 slice. The times are simulated.
32 devices in a mesh: sp: 8 (over z, y), tp: 4 (over x, core).
Axes of the slice: x: 2, y: 2, z: 4, core: 2. Of those that a mesh axis runs over, the one named last changes fastest.
Arguments:
- stream: bfloat16 [4096, 2048], P('sp', 'tp'), may hold values from -6 to 6
- doc_ids: int32 [4096], P('sp'), may hold values from 0 to 3, never falling along the last dimension, each value on 1 to 2304 neighbouring positions
- norm_gain: float32 [2, 2048], replicated, may hold values from 0.1 to 1.9
- gate_proj: bfloat16 [2, 2048, 2048], P(None, 'sp', 'tp'), may hold values from -0.125 to 0.125
- input_gate: bfloat16 [2, 2048, 2048], P(None, 'sp', 'tp'), may hold values from -0.125 to 0.125
- value_proj: bfloat16 [2, 2048, 2048], P(None, 'sp', 'tp'), may hold values from -0.125 to 0.125
- taps: float32 [2, 3, 2048], P(None, None, 'tp'), may hold values from -3 to 3
- out_proj: bfloat16 [2, 2048, 2048], P(None, 'tp', 'sp'), may hold values from -0.125 to 0.125
Outputs:
- result: bfloat16 [4096, 2048], P('sp', 'tp')
Inputs may be any that keep to these rules, and one draw needn't show every extreme that they name: `doc_ids`: document numbers never fall along the sequence; each document holds 1 to 2304 positions.
All inputs are finite; a program needn't handle non-finite values.
Results may differ from a plain program's by a relative error of at most 0.03.
Values may be sent and summed in bfloat16 or wider, within the bound.
A program may use at most 64 MiB of HBM per device.

v0:
```python
import jax
import jax.numpy as jnp
from jax import lax
from jax.sharding import PartitionSpec as P

epsilon = 1e-06


def with_halo(value, sides, width):
    for axis, dim in sides:
        size, length = (lax.axis_size(axis), value.shape[dim])
        up = [(i, (i + 1) % size) for i in range(size - 1)]
        down = [(j, i) for i, j in up]
        last = lax.slice_in_dim(value, length - width, length, axis=dim)
        leading = lax.slice_in_dim(value, 0, width, axis=dim)
        before = lax.ppermute(last, axis, up)
        after = lax.ppermute(leading, axis, down)
        value = jnp.concatenate([before, value, after], axis=dim)
    return value


def per_device(stream, doc_ids, norm_gain, gate_proj, input_gate, value_proj, taps, out_proj):
    layers = gate_proj.shape[0]
    gathered_in = (
        lax.all_gather(gate_proj, "sp", axis=1, tiled=True),
        lax.all_gather(input_gate, "sp", axis=1, tiled=True),
        lax.all_gather(value_proj, "sp", axis=1, tiled=True),
    )
    gathered_out = lax.all_gather(out_proj, "sp", axis=2, tiled=True)
    current = stream
    for layer_index in range(layers):
        full_rows = lax.all_gather(current, "tp", axis=1, tiled=True)
        widened = full_rows.astype(jnp.float32)
        scale = lax.rsqrt(jnp.mean(widened * widened, axis=-1, keepdims=True) + epsilon)
        normed = (widened * scale * norm_gain[layer_index]).astype(jnp.bfloat16)
        gate_b = jnp.dot(normed, gathered_in[0][layer_index], preferred_element_type=jnp.float32)
        gate_c = jnp.dot(normed, gathered_in[1][layer_index], preferred_element_type=jnp.float32)
        values = jnp.dot(normed, gathered_in[2][layer_index], preferred_element_type=jnp.float32)
        gate_b = gate_b.astype(jnp.bfloat16)
        gate_c = gate_c.astype(jnp.bfloat16)
        values = values.astype(jnp.bfloat16)
        mixed_in = (gate_c.astype(jnp.float32) * values.astype(jnp.float32)).astype(jnp.bfloat16)
        padded, doc_padded = (
            with_halo(mixed_in, (("sp", 0),), 1),
            with_halo(doc_ids, (("sp", 0),), 1),
        )
        same_prev = (doc_padded[:-2] == doc_ids)[:, None]
        same_next = (doc_padded[2:] == doc_ids)[:, None]
        kernel_taps = taps[layer_index]
        convolved = (
            jnp.where(same_prev, kernel_taps[0] * padded[:-2].astype(jnp.float32), 0.0)
            + kernel_taps[1] * mixed_in.astype(jnp.float32)
            + jnp.where(same_next, kernel_taps[2] * padded[2:].astype(jnp.float32), 0.0)
        )
        gated = (gate_b.astype(jnp.float32) * convolved).astype(jnp.bfloat16)
        partials = jnp.dot(gated, gathered_out[layer_index], preferred_element_type=jnp.float32)
        summed = lax.psum_scatter(
            partials.astype(jnp.bfloat16), "tp", scatter_dimension=1, tiled=True
        ).astype(jnp.float32)
        current = (current.astype(jnp.float32) + summed).astype(jnp.bfloat16)
    return current


def solution(mesh):
    in_specs = (
        P("sp", "tp"),
        P("sp"),
        P(),
        P(None, "sp", "tp"),
        P(None, "sp", "tp"),
        P(None, "sp", "tp"),
        P(None, None, "tp"),
        P(None, "tp", "sp"),
    )
    out_specs = P("sp", "tp")
    return jax.shard_map(
        per_device, mesh=mesh, in_specs=in_specs, out_specs=out_specs, check_vma=False
    )
```

profile of v0, /device:TPU:0, one launch (start us, length us, event | category | flops | bytes accessed | tf_op | source)
XLA Modules:
  0.0 454.6 jit_solution(15519410524372381653)
XLA Ops:
  6.5 0.0 all-gather.7.cloned.1.call-start
  6.5 0.7 all-gather.7.cloned.1.call-update
  7.3 0.0 all-gather.13.cloned.1.call-start
  7.3 0.7 all-gather.13.cloned.1.call-update
  8.0 0.0 all-gather.11.cloned.1.call-start
  8.1 0.7 all-gather.11.cloned.1.call-update
  8.7 0.0 all-gather.9.cloned.1.call-start
  8.8 0.5 all-gather.9.cloned.1.call-update
  9.3 0.0 all-gather.15.cloned.1.call-start
  9.4 0.5 all-gather.15.cloned.1.call-update
  9.9 0.0 reduce-scatter.3.cloned.1.call-start
  9.9 1.3 fusion.64
  11.3 5.4 %collective-permute-start = (s32[1]{0:T(128)}, s32[1]{0:T(128)}, u32[]{:S(2)}, u32[]{:S(2)}) collective-permute-start(s32[1]{0:T(128)} %get-tuple-element.21), channel_id=1, source_target_pairs={{0,4},{4,8},{8,12},{12,16},{16,20},{20,24},{24,28},{1,5},{5,9},{9,... | collective-permute-start | bytes 20 | tf_op jit(solution)/shard_map/ppermute | solution.py:16
  16.7 1.3 collective-permute-start.2
  18.0 0.8 fusion.63
  18.8 0.8 fusion.62
  19.6 0.0 collective-permute-done
  19.6 2.5 collective-permute-done.2
  22.2 2.1 pad_add_fusion
  24.3 9.9 %all-gather.7.cloned.1.call-done = bf16[512,2048]{1,0:T(8,128)(2,1)} async-done(((bf16[512,512]{1,0:T(8,128)(2,1)}), bf16[512,2048]{1,0:T(8,128)(2,1)}) %all-gather.7.cloned.1.call-update) | async-done | bytes 2097168 | tf_op jit(solution)/shard_map/all_gather | solution.py:32
  34.2 2.1 fusion
  36.3 72.9 %all-gather.13.cloned.1.call-done = bf16[2,2048,512]{2,1,0:T(8,128)(2,1)} async-done(((bf16[2,256,512]{2,1,0:T(8,128)(2,1)}), bf16[2,2048,512]{2,1,0:T(8,128)(2,1)}) %all-gather.13.cloned.1.call-update) | async-done | bytes 4194320 | tf_op jit(solution)/shard_map/all_gather | solution.py:27
  109.2 0.0 copy-start.2
  109.2 4.7 %fusion.19 = f32[512,512]{1,0:T(8,128)} fusion(bf16[2,2048,512]{2,1,0:T(8,128)(2,1)} %all-gather.13.cloned.1.call-done, bf16[512,2048]{1,0:T(8,128)(2,1)} %all-gather.7.cloned.1.call-done, f32[2048]{0:T(1024)S(1)} %bitcast.79, f32[512]{0:T(512)S(1)} %add_rsqrt_fusion.1), kind=kOutput, calls=%fused_computation.33 | convolution fusion | flops 1078460416 | bytes 5253120 | tf_op jit(solution)/shard_map/dot_general | solution.py:38
  113.9 0.0 copy-start.4
  113.9 68.9 %all-gather.11.cloned.1.call-done = bf16[2,2048,512]{2,1,0:T(8,128)(2,1)} async-done(((bf16[2,256,512]{2,1,0:T(8,128)(2,1)}), bf16[2,2048,512]{2,1,0:T(8,128)(2,1)}) %all-gather.11.cloned.1.call-update) | async-done | bytes 4194320 | tf_op jit(solution)/shard_map/all_gather | solution.py:26
  182.7 0.0 copy-done.2
  182.7 3.1 fusion.30
  185.9 2.5 collective-permute-start.1
  188.4 1.3 collective-permute-start.3
  189.7 0.0 copy-done.4
  189.7 0.1 slice_compare_fusion.1
  189.8 66.4 %all-gather.9.cloned.1.call-done = bf16[2,2048,512]{2,1,0:T(8,128)(2,1)} async-done(((bf16[2,256,512]{2,1,0:T(8,128)(2,1)}), bf16[2,2048,512]{2,1,0:T(8,128)(2,1)}) %all-gather.9.cloned.1.call-update) | async-done | bytes 4194320 | tf_op jit(solution)/shard_map/all_gather | solution.py:25
  256.1 75.1 %all-gather.15.cloned.1.call-done = bf16[2,512,2048]{2,1,0:T(8,128)(2,1)} async-done(((bf16[2,512,256]{2,1,0:T(8,128)(2,1)}), bf16[2,512,2048]{2,1,0:T(8,128)(2,1)}) %all-gather.15.cloned.1.call-update) | async-done | bytes 4194320 | tf_op jit(solution)/shard_map/all_gather | solution.py:29
  331.2 0.0 collective-permute-done.1
  331.2 0.0 collective-permute-done.3
  331.2 0.0 copy-start.1
  331.2 6.3 %convolution_convert_fusion.1 = bf16[512,2048]{1,0:T(8,128)(2,1)} fusion(bf16[2,512,2048]{2,1,0:T(8,128)(2,1)} %all-gather.15.cloned.1.call-done, bf16[2,2048,512]{2,1,0:T(8,128)(2,1)} %all-gather.9.cloned.1.call-done, bf16[512,512]{1,0:T(8,128)(2,1)S(1)} %fusion.30, bf16[1,512]{1,0:T(2,128)(2,1)S(1)} %collective-permute-done.3, ...), kind=kOutput, calls=%fused_computation.11 | convolution fusion | flops 2157969408 | bytes 8932352 | tf_op jit(solution)/shard_map/dot_general | solution.py:56
  337.5 0.0 reduce-scatter.3.cloned.1.call-update
  337.6 0.0 all-gather.17.cloned.1.call-start
  337.6 29.4 %reduce-scatter.3.cloned.1.call-done = bf16[512,512]{1,0:T(8,128)(2,1)} async-done(((bf16[512,2048]{1,0:T(8,128)(2,1)}), bf16[512,512]{1,0:T(8,128)(2,1)}) %reduce-scatter.3.cloned.1.call-update) | async-done | bytes 524304 | tf_op jit(solution)/shard_map/reduce_scatter | solution.py:57
  367.0 0.0 copy-done.1
  367.1 2.0 add_convert_fusion.1
  369.0 0.0 all-gather.17.cloned.1.call-update
  369.0 0.0 reduce-scatter.5.cloned.1.call-start
  369.1 22.7 %all-gather.17.cloned.1.call-done = bf16[512,2048]{1,0:T(8,128)(2,1)} async-done(((bf16[512,512]{1,0:T(8,128)(2,1)}), bf16[512,2048]{1,0:T(8,128)(2,1)}) %all-gather.17.cloned.1.call-update) | async-done | bytes 2097168 | tf_op jit(solution)/shard_map/all_gather | solution.py:32
  391.8 2.1 fusion.3
  393.8 0.0 copy-start.3
  393.8 0.0 copy-start.5
  393.9 3.7 fusion.27
  397.5 0.0 copy-done.3
  397.5 0.4 copy-done.5
  397.9 1.3 fusion.28
  399.2 3.4 collective-permute-start.4
  402.6 1.3 collective-permute-start.5
  403.9 0.0 collective-permute-done.4
  403.9 4.2 collective-permute-done.5
  408.1 0.0 copy-start
  408.1 6.3 %convolution_convert_fusion = bf16[512,2048]{1,0:T(8,128)(2,1)} fusion(bf16[2,512,2048]{2,1,0:T(8,128)(2,1)} %all-gather.15.cloned.1.call-done, bf16[2,2048,512]{2,1,0:T(8,128)(2,1)} %all-gather.9.cloned.1.call-done, bf16[512,512]{1,0:T(8,128)(2,1)S(1)} %fusion.28, bf16[1,512]{1,0:T(2,128)(2,1)S(1)} %collective-permute-done.5, ...), kind=kOutput, calls=%fused_computation.10 | convolution fusion | flops 2157969408 | bytes 8932352 | tf_op jit(solution)/shard_map/dot_general | solution.py:56
  414.4 0.0 reduce-scatter.5.cloned.1.call-update
  414.5 31.3 %reduce-scatter.5.cloned.1.call-done = bf16[512,512]{1,0:T(8,128)(2,1)} async-done(((bf16[512,2048]{1,0:T(8,128)(2,1)}), bf16[512,512]{1,0:T(8,128)(2,1)}) %reduce-scatter.5.cloned.1.call-update) | async-done | bytes 524304 | tf_op jit(solution)/shard_map/reduce_scatter | solution.py:57
  445.8 0.0 copy-done
  445.8 2.0 add_convert_fusion
  (4 shorter events, 0.0 us)
Async XLA Ops:
  6.5 27.7 %all-gather.7.cloned.1.call-start = ((), (), s32[]{:S(2)}) async-start(), calls=%async_computation.2 | async-start | bytes 2621440 | tf_op jit(solution)/shard_map/all_gather | solution.py:32
  7.3 101.9 %all-gather.13.cloned.1.call-start = ((), (), s32[]{:S(2)}) async-start(), calls=%async_computation.5 | async-start | bytes 4718592 | tf_op jit(solution)/shard_map/all_gather | solution.py:27
  8.0 174.7 %all-gather.11.cloned.1.call-start = ((), (), s32[]{:S(2)}) async-start(), calls=%async_computation.4 | async-start | bytes 4718592 | tf_op jit(solution)/shard_map/all_gather | solution.py:26
  8.7 247.4 %all-gather.9.cloned.1.call-start = ((), (), s32[]{:S(2)}) async-start(), calls=%async_computation.3 | async-start | bytes 4718592 | tf_op jit(solution)/shard_map/all_gather | solution.py:25
  9.3 321.9 %all-gather.15.cloned.1.call-start = ((), (), s32[]{:S(2)}) async-start(), calls=%async_computation.6 | async-start | bytes 4718592 | tf_op jit(solution)/shard_map/all_gather | solution.py:29
  9.9 357.1 %reduce-scatter.3.cloned.1.call-start = ((), (), s32[]{:S(2)}) async-start(), calls=%async_computation.7 | async-start | bytes 2621440 | tf_op jit(solution)/shard_map/reduce_scatter | solution.py:57
  11.3 8.3 %collective-permute-start = (s32[1]{0:T(128)}, s32[1]{0:T(128)}, u32[]{:S(2)}, u32[]{:S(2)}) collective-permute-start(s32[1]{0:T(128)} %get-tuple-element.21), channel_id=1, source_target_pairs={{0,4},{4,8},{8,12},{12,16},{16,20},{20,24},{24,28},{1,5},{5,9},{9,... | collective-permute-start | bytes 20 | tf_op jit(solution)/shard_map/ppermute | solution.py:16
  16.7 5.5 %collective-permute-start.2 = (s32[1]{0:T(128)}, s32[1]{0:T(128)}, u32[]{:S(2)}, u32[]{:S(2)}) collective-permute-start(s32[1]{0:T(128)} %get-tuple-element.22), channel_id=1, source_target_pairs={{4,0},{8,4},{12,8},{16,12},{20,16},{24,20},{28,24},{5,1},{9,5},{13... | collective-permute-start | bytes 20 | tf_op jit(solution)/shard_map/ppermute | solution.py:17
  109.2 73.5 %copy-start.2 = (bf16[512,2048]{1,0:T(8,128)(2,1)S(1)}, bf16[512,2048]{1,0:T(8,128)(2,1)}, u32[]{:S(2)}) copy-start(bf16[512,2048]{1,0:T(8,128)(2,1)} %all-gather.7.cloned.1.call-done) | copy-start | bytes 6291460
  113.9 75.8 %copy-start.4 = (s32[512]{0:T(512)S(1)}, s32[512]{0:T(512)}, u32[]{:S(2)}) copy-start(s32[512]{0:T(512)} %param.9) | copy-start | bytes 6148
  185.9 145.3 %collective-permute-start.1 = (bf16[1,512]{1,0:T(2,128)(2,1)S(1)}, bf16[1,512]{1,0:T(2,128)(2,1)S(1)}, u32[]{:S(2)}, u32[]{:S(2)}) collective-permute-start(bf16[1,512]{1,0:T(2,128)(2,1)S(1)} %get-tuple-element.7), channel_id=1, source_target_pairs={{0,4},{4,8},{8,12},{12,16},{16,20},{20,24},{24,28},{1,5},{5,9},{9,... | collective-permute-start | bytes 3080 | tf_op jit(solution)/shard_map/ppermute | solution.py:16
  188.4 142.8 %collective-permute-start.3 = (bf16[1,512]{1,0:T(2,128)(2,1)S(1)}, bf16[1,512]{1,0:T(2,128)(2,1)S(1)}, u32[]{:S(2)}, u32[]{:S(2)}) collective-permute-start(bf16[1,512]{1,0:T(2,128)(2,1)S(1)} %get-tuple-element.8), channel_id=1, source_target_pairs={{4,0},{8,4},{12,8},{16,12},{20,16},{24,20},{28,24},{5,1},{9,5},{13... | collective-permute-start | bytes 3080 | tf_op jit(solution)/shard_map/ppermute | solution.py:17
  331.2 35.8 %copy-start.1 = (bf16[512,512]{1,0:T(8,128)(2,1)S(1)}, bf16[512,512]{1,0:T(8,128)(2,1)}, u32[]{:S(2)}) copy-start(bf16[512,512]{1,0:T(8,128)(2,1)} %param.8) | copy-start | bytes 1572868
  337.6 54.2 %all-gather.17.cloned.1.call-start = ((), (), s32[]{:S(2)}) async-start(), calls=%async_computation.8 | async-start | bytes 2621440 | tf_op jit(solution)/shard_map/all_gather | solution.py:32
  369.0 76.7 %reduce-scatter.5.cloned.1.call-start = ((), (), s32[]{:S(2)}) async-start(), calls=%async_computation.9 | async-start | bytes 2621440 | tf_op jit(solution)/shard_map/reduce_scatter | solution.py:57
  393.8 3.7 copy-start.3
  393.8 4.1 copy-start.5
  399.2 4.7 %collective-permute-start.4 = (bf16[1,512]{1,0:T(2,128)(2,1)S(1)}, bf16[1,512]{1,0:T(2,128)(2,1)S(1)}, u32[]{:S(2)}, u32[]{:S(2)}) collective-permute-start(bf16[1,512]{1,0:T(2,128)(2,1)S(1)} %get-tuple-element.5), channel_id=1, source_target_pairs={{0,4},{4,8},{8,12},{12,16},{16,20},{20,24},{24,28},{1,5},{5,9},{9,... | collective-permute-start | bytes 3080 | tf_op jit(solution)/shard_map/ppermute | solution.py:16
  402.6 5.5 %collective-permute-start.5 = (bf16[1,512]{1,0:T(2,128)(2,1)S(1)}, bf16[1,512]{1,0:T(2,128)(2,1)S(1)}, u32[]{:S(2)}, u32[]{:S(2)}) collective-permute-start(bf16[1,512]{1,0:T(2,128)(2,1)S(1)} %get-tuple-element.6), channel_id=1, source_target_pairs={{4,0},{8,4},{12,8},{16,12},{20,16},{24,20},{28,24},{5,1},{9,5},{13... | collective-permute-start | bytes 3080 | tf_op jit(solution)/shard_map/ppermute | solution.py:17
  408.1 37.7 %copy-start = (bf16[512,512]{1,0:T(8,128)(2,1)S(1)}, bf16[512,512]{1,0:T(8,128)(2,1)}, u32[]{:S(2)}) copy-start(bf16[512,512]{1,0:T(8,128)(2,1)} %add_convert_fusion.1) | copy-start | bytes 1572868
Sparse Core Ops, SparseCore 0:
  8.9 25.2 all-gather.6
  36.4 72.7 all-gather.12
  111.4 71.2 all-gather.10
  184.8 71.2 all-gather.8
  258.0 73.1 all-gather.14
  337.7 29.3 reduce-scatter.2
  369.2 22.5 all-gather.16
  414.6 31.1 reduce-scatter.4
where the time goes:
time: 455 us
  waiting for transfers between devices  386 us (85%)
  matrix products  25.4 us (6%)
  starting transfers between devices  15.4 us (3%)
  between operations  13.6 us (3%)
  other arithmetic  10.3 us (2%)
    all_gather x1, waiting for transfers between devices, per_device(): gathered_out = lax.all_gather(out_proj, 'sp', axis=2, tiled=True)  75.1 us
    all_gather x1, waiting for transfers between devices, per_device(): lax.all_gather(value_proj, 'sp', axis=1, tiled=True)  72.9 us
    all_gather x1, waiting for transfers between devices, per_device(): lax.all_gather(input_gate, 'sp', axis=1, tiled=True)  68.9 us
    all_gather x1, waiting for transfers between devices, per_device(): lax.all_gather(gate_proj, 'sp', axis=1, tiled=True)  66.4 us
    reduce_scatter x2, waiting for transfers between devices, per_device(): lax.psum_scatter(partials.astype(jnp.bfloat16), 'tp', scatter_dimension=1...  60.7 us
    all_gather x2, waiting for transfers between devices, per_device(): full_rows = lax.all_gather(current, 'tp', axis=1, tiled=True)  32.6 us
    dot_general x2, matrix products, per_device(): jnp.dot(gated, gathered_out[layer_index], preferred_element_type=jnp.floa...  12.7 us
    ppermute x3, starting transfers between devices, with_halo(): before = lax.ppermute(last, axis, up)  11.2 us
  transfers between devices with their start and end apart: 14, of which 10 were waited for; matrix products, arithmetic and copies ran while one was open for 3% of the time, Pallas kernels for 0%

commit v1 on v0

--- a/solution.py
+++ b/solution.py
@@ -2,6 +2,7 @@
 import jax.numpy as jnp
 from jax import lax
 from jax.sharding import PartitionSpec as P
+from jax.lax import all_gather
 
 epsilon = 1e-06
 
@@ -26,7 +27,8 @@
         lax.all_gather(input_gate, "sp", axis=1, tiled=True),
         lax.all_gather(value_proj, "sp", axis=1, tiled=True),
     )
-    gathered_out = lax.all_gather(out_proj, "sp", axis=2, tiled=True)
+    track_cycles_by_axis = lambda my_data: jnp.concatenate(all_gather(my_data, "sp"), axis=2)
+    gathered_out = track_cycles_by_axis(out_proj)
     current = stream
     for layer_index in range(layers):
         full_rows = lax.all_gather(current, "tp", axis=1, tiled=True)

time: 455 us -> 454 us (level)
  waiting for transfers between devices: 386 us -> 378 us
  local copies, waits for them, and re-layouts: 3.38 us -> 10.9 us
    slice x0 -> x3, local copies, waits for them, and re-layouts: none -> 10.3 us  [per_device(): gathered_out[layer_index]]
    all_gather x1, waiting for transfers between devices: 75.1 us -> 66.4 us  [per_device(): all_gather(my_data, 'sp')]
  transfers between devices with their start and end apart: 14 -> 14, of which waited for: 10 -> 10; matrix products, arithmetic and copies ran while one was open for 3% -> 5% of each run, Pallas kernels for 0% -> 0%
where the time goes in v1:
time: 454 us; the launch traced here: 453 us
  waiting for transfers between devices  378 us (83%)
  matrix products  25.1 us (6%)
  starting transfers between devices  15.4 us (3%)
  between operations  13.7 us (3%)
  local copies, waits for them, and re-layouts  10.9 us (2%)
  other arithmetic  9.91 us (2%)
    all_gather x1, waiting for transfers between devices, per_device(): lax.all_gather(value_proj, 'sp', axis=1, tiled=True)  72.8 us
    all_gather x1, waiting for transfers between devices, per_device(): lax.all_gather(input_gate, 'sp', axis=1, tiled=True)  69.6 us
    all_gather x1, waiting for transfers between devices, per_device(): all_gather(my_data, 'sp')  66.4 us
    all_gather x1, waiting for transfers between devices, per_device(): lax.all_gather(gate_proj, 'sp', axis=1, tiled=True)  65.5 us
    reduce_scatter x2, waiting for transfers between devices, per_device(): lax.psum_scatter(partials.astype(jnp.bfloat16), 'tp', scatter_dimension=1...  61.1 us
    all_gather x2, waiting for transfers between devices, per_device(): full_rows = lax.all_gather(current, 'tp', axis=1, tiled=True)  33.7 us
    dot_general x2, matrix products, per_device(): jnp.dot(gated, gathered_out[layer_index], preferred_element_type=jnp.floa...  13.7 us
    ppermute x3, starting transfers between devices, with_halo(): before = lax.ppermute(last, axis, up)  11.3 us
  transfers between devices with their start and end apart: 14, of which 10 were waited for; matrix products, arithmetic and copies ran while one was open for 5% of the time, Pallas kernels for 0%

profile of v1, /device:TPU:0, one launch (start us, length us, event | category | flops | bytes accessed | tf_op | source)
XLA Modules:
  0.0 453.4 jit_solution(7753369005543131244)
XLA Ops:
  6.5 0.0 copy-start.5
  6.5 0.0 copy-start.6
  6.5 0.0 all-gather.8.cloned.1.call-start
  6.5 0.7 all-gather.8.cloned.1.call-update
  7.3 0.0 all-gather.14.cloned.1.call-start
  7.3 0.7 all-gather.14.cloned.1.call-update
  8.0 0.0 all-gather.12.cloned.1.call-start
  8.1 0.7 all-gather.12.cloned.1.call-update
  8.7 0.0 all-gather.18.cloned.1.call-start
  8.8 0.5 all-gather.18.cloned.1.call-update
  9.3 0.0 all-gather.10.cloned.1.call-start
  9.4 0.5 all-gather.10.cloned.1.call-update
  9.9 0.0 reduce-scatter.3.cloned.1.call-start
  10.0 0.0 copy-done.5
  10.0 0.6 fusion.65
  10.6 5.5 %collective-permute-start = (s32[1]{0:T(128)}, s32[1]{0:T(128)}, u32[]{:S(2)}, u32[]{:S(2)}) collective-permute-start(s32[1]{0:T(128)} %get-tuple-element.23), channel_id=1, source_target_pairs={{0,4},{4,8},{8,12},{12,16},{16,20},{20,24},{24,28},{1,5},{5,9},{9,... | collective-permute-start | bytes 20 | tf_op jit(solution)/shard_map/ppermute | solution.py:17
  16.0 1.3 collective-permute-start.2
  17.3 0.0 copy-done.6
  17.3 0.0 copy-done.4
  17.4 0.0 collective-permute-done
  17.4 4.3 collective-permute-done.2
  21.6 1.4 pad_add_fusion
  23.1 0.1 slice_compare_fusion.1
  23.2 11.1 %all-gather.8.cloned.1.call-done = bf16[512,2048]{1,0:T(8,128)(2,1)} async-done(((bf16[512,512]{1,0:T(8,128)(2,1)}), bf16[512,2048]{1,0:T(8,128)(2,1)}) %all-gather.8.cloned.1.call-update) | async-done | bytes 2097168 | tf_op jit(solution)/shard_map/all_gather | solution.py:34
  34.2 0.0 copy-start.2
  34.2 2.2 fusion
  36.5 72.8 %all-gather.14.cloned.1.call-done = bf16[2,2048,512]{2,1,0:T(8,128)(2,1)} async-done(((bf16[2,256,512]{2,1,0:T(8,128)(2,1)}), bf16[2,2048,512]{2,1,0:T(8,128)(2,1)}) %all-gather.14.cloned.1.call-update) | async-done | bytes 4194320 | tf_op jit(solution)/shard_map/all_gather | solution.py:28
  109.2 0.0 copy-done.2
  109.2 3.9 fusion.19
  113.1 69.6 %all-gather.12.cloned.1.call-done = bf16[2,2048,512]{2,1,0:T(8,128)(2,1)} async-done(((bf16[2,256,512]{2,1,0:T(8,128)(2,1)}), bf16[2,2048,512]{2,1,0:T(8,128)(2,1)}) %all-gather.12.cloned.1.call-update) | async-done | bytes 4194320 | tf_op jit(solution)/shard_map/all_gather | solution.py:27
  182.7 3.2 fusion.30
  185.9 2.4 collective-permute-start.1
  188.4 1.3 collective-permute-start.3
  189.7 66.4 %all-gather.18.cloned.1.call-done = bf16[16,512,256]{2,1,0:T(8,128)(2,1)} async-done(((bf16[2,512,256]{2,1,0:T(8,128)(2,1)}), bf16[16,512,256]{2,1,0:T(8,128)(2,1)}) %all-gather.18.cloned.1.call-update) | async-done | bytes 4194320 | tf_op jit(solution)/shard_map/all_gather | solution.py:30
  256.1 3.9 fusion.60
  260.0 3.9 copy.11
  263.9 65.5 %all-gather.10.cloned.1.call-done = bf16[2,2048,512]{2,1,0:T(8,128)(2,1)} async-done(((bf16[2,256,512]{2,1,0:T(8,128)(2,1)}), bf16[2,2048,512]{2,1,0:T(8,128)(2,1)}) %all-gather.10.cloned.1.call-update) | async-done | bytes 4194320 | tf_op jit(solution)/shard_map/all_gather | solution.py:26
  329.5 0.0 collective-permute-done.1
  329.5 0.0 collective-permute-done.3
  329.5 6.8 %convolution_convert_fusion.1 = bf16[512,2048]{1,0:T(8,128)(2,1)} fusion(bf16[512,2048]{0,1:T(8,128)(2,1)} %bitcast.78, bf16[2,2048,512]{2,1,0:T(8,128)(2,1)} %all-gather.10.cloned.1.call-done, bf16[512,512]{1,0:T(8,128)(2,1)S(1)} %fusion.30, bf16[1,512]{1,0:T(2,128)(2,1)S(1)} %collective-permute-done.3, bf16[1,512]{1,0:T(2,128)(2,1)S(1)} %collective-permute-done.1, ...), kind=kOutput, calls=%fused_computation.11 | convolution fusion | flops 2157969408 | bytes 8932352 | tf_op jit(solution)/shard_map/dot_general | solution.py:58
  336.3 0.0 reduce-scatter.3.cloned.1.call-update
  336.3 0.0 all-gather.16.cloned.1.call-start
  336.4 29.8 %reduce-scatter.3.cloned.1.call-done = bf16[512,512]{1,0:T(8,128)(2,1)} async-done(((bf16[512,2048]{1,0:T(8,128)(2,1)}), bf16[512,512]{1,0:T(8,128)(2,1)}) %reduce-scatter.3.cloned.1.call-update) | async-done | bytes 524304 | tf_op jit(solution)/shard_map/reduce_scatter | solution.py:59
  366.2 0.0 copy-done.1
  366.2 2.0 add_convert_fusion.1
  368.2 0.0 all-gather.16.cloned.1.call-update
  368.2 0.0 reduce-scatter.5.cloned.1.call-start
  368.2 22.7 %all-gather.16.cloned.1.call-done = bf16[512,2048]{1,0:T(8,128)(2,1)} async-done(((bf16[512,512]{1,0:T(8,128)(2,1)}), bf16[512,2048]{1,0:T(8,128)(2,1)}) %all-gather.16.cloned.1.call-update) | async-done | bytes 2097168 | tf_op jit(solution)/shard_map/all_gather | solution.py:34
  390.9 2.2 fusion.3
  393.1 0.0 copy-done.3
  393.1 0.0 copy-start.7
  393.1 3.0 fusion.27
  396.2 0.0 copy-done.7
  396.2 1.3 fusion.28
  397.5 3.4 collective-permute-start.4
  400.9 1.3 collective-permute-start.5
  402.2 2.5 copy.12
  404.6 0.0 collective-permute-done.4
  404.6 1.7 collective-permute-done.5
  406.4 6.9 %convolution_convert_fusion = bf16[512,2048]{1,0:T(8,128)(2,1)} fusion(bf16[512,2048]{0,1:T(8,128)(2,1)} %bitcast.79, bf16[2,2048,512]{2,1,0:T(8,128)(2,1)} %all-gather.10.cloned.1.call-done, bf16[512,512]{1,0:T(8,128)(2,1)S(1)} %fusion.28, bf16[1,512]{1,0:T(2,128)(2,1)S(1)} %collective-permute-done.5, bf16[1,512]{1,0:T(2,128)(2,1)S(1)} %collective-permute-done.4, ...), kind=kOutput, calls=%fused_computation.10 | convolution fusion | flops 2157969408 | bytes 8932352 | tf_op jit(solution)/shard_map/dot_general | solution.py:58
  413.3 0.0 reduce-scatter.5.cloned.1.call-update
  413.3 31.3 %reduce-scatter.5.cloned.1.call-done = bf16[512,512]{1,0:T(8,128)(2,1)} async-done(((bf16[512,2048]{1,0:T(8,128)(2,1)}), bf16[512,512]{1,0:T(8,128)(2,1)}) %reduce-scatter.5.cloned.1.call-update) | async-done | bytes 524304 | tf_op jit(solution)/shard_map/reduce_scatter | solution.py:59
  444.6 0.0 copy-done
  444.6 2.0 add_convert_fusion
  (10 shorter events, 0.1 us)
Async XLA Ops:
  6.5 3.4 copy-start.5
  6.5 10.8 %copy-start.6 = (f32[2,3,512]{2,0,1:T(2,128)S(1)}, f32[2,3,512]{2,0,1:T(2,128)}, u32[]{:S(2)}) copy-start(f32[2,3,512]{2,0,1:T(2,128)} %param.14) | copy-start | bytes 36868
  6.5 10.8 %copy-start.4 = (f32[2,2048]{1,0:T(2,128)S(1)}, f32[2,2048]{1,0:T(2,128)}, u32[]{:S(2)}) copy-start(f32[2,2048]{1,0:T(2,128)} %param.10) | copy-start | bytes 49156
  6.5 27.7 %all-gather.8.cloned.1.call-start = ((), (), s32[]{:S(2)}) async-start(), calls=%async_computation.2 | async-start | bytes 2621440 | tf_op jit(solution)/shard_map/all_gather | solution.py:34
  7.3 101.9 %all-gather.14.cloned.1.call-start = ((), (), s32[]{:S(2)}) async-start(), calls=%async_computation.5 | async-start | bytes 4718592 | tf_op jit(solution)/shard_map/all_gather | solution.py:28
  8.0 174.7 %all-gather.12.cloned.1.call-start = ((), (), s32[]{:S(2)}) async-start(), calls=%async_computation.4 | async-start | bytes 4718592 | tf_op jit(solution)/shard_map/all_gather | solution.py:27
  8.7 247.3 %all-gather.18.cloned.1.call-start = ((), (), s32[]{:S(2)}) async-start(), calls=%async_computation.9 | async-start | bytes 4718592 | tf_op jit(solution)/shard_map/all_gather | solution.py:30
  9.3 320.1 %all-gather.10.cloned.1.call-start = ((), (), s32[]{:S(2)}) async-start(), calls=%async_computation.3 | async-start | bytes 4718592 | tf_op jit(solution)/shard_map/all_gather | solution.py:26
  9.9 356.3 %reduce-scatter.3.cloned.1.call-start = ((), (), s32[]{:S(2)}) async-start(), calls=%async_computation.6 | async-start | bytes 2621440 | tf_op jit(solution)/shard_map/reduce_scatter | solution.py:59
  10.6 6.8 %collective-permute-start = (s32[1]{0:T(128)}, s32[1]{0:T(128)}, u32[]{:S(2)}, u32[]{:S(2)}) collective-permute-start(s32[1]{0:T(128)} %get-tuple-element.23), channel_id=1, source_target_pairs={{0,4},{4,8},{8,12},{12,16},{16,20},{20,24},{24,28},{1,5},{5,9},{9,... | collective-permute-start | bytes 20 | tf_op jit(solution)/shard_map/ppermute | solution.py:17
  16.0 5.6 %collective-permute-start.2 = (s32[1]{0:T(128)}, s32[1]{0:T(128)}, u32[]{:S(2)}, u32[]{:S(2)}) collective-permute-start(s32[1]{0:T(128)} %get-tuple-element.24), channel_id=1, source_target_pairs={{4,0},{8,4},{12,8},{16,12},{20,16},{24,20},{28,24},{5,1},{9,5},{13... | collective-permute-start | bytes 20 | tf_op jit(solution)/shard_map/ppermute | solution.py:18
  34.2 75.0 %copy-start.2 = (bf16[512,2048]{1,0:T(8,128)(2,1)S(1)}, bf16[512,2048]{1,0:T(8,128)(2,1)}, u32[]{:S(2)}) copy-start(bf16[512,2048]{1,0:T(8,128)(2,1)} %all-gather.8.cloned.1.call-done) | copy-start | bytes 6291460
  185.9 143.5 %collective-permute-start.1 = (bf16[1,512]{1,0:T(2,128)(2,1)S(1)}, bf16[1,512]{1,0:T(2,128)(2,1)S(1)}, u32[]{:S(2)}, u32[]{:S(2)}) collective-permute-start(bf16[1,512]{1,0:T(2,128)(2,1)S(1)} %get-tuple-element.9), channel_id=1, source_target_pairs={{0,4},{4,8},{8,12},{12,16},{16,20},{20,24},{24,28},{1,5},{5,9},{9,... | collective-permute-start | bytes 3080 | tf_op jit(solution)/shard_map/ppermute | solution.py:17
  188.4 141.1 %collective-permute-start.3 = (bf16[1,512]{1,0:T(2,128)(2,1)S(1)}, bf16[1,512]{1,0:T(2,128)(2,1)S(1)}, u32[]{:S(2)}, u32[]{:S(2)}) collective-permute-start(bf16[1,512]{1,0:T(2,128)(2,1)S(1)} %get-tuple-element.10), channel_id=1, source_target_pairs={{4,0},{8,4},{12,8},{16,12},{20,16},{24,20},{28,24},{5,1},{9,5},{13... | collective-permute-start | bytes 3080 | tf_op jit(solution)/shard_map/ppermute | solution.py:18
  336.3 29.9 %copy-start.1 = (bf16[512,512]{1,0:T(8,128)(2,1)S(1)}, bf16[512,512]{1,0:T(8,128)(2,1)}, u32[]{:S(2)}) copy-start(bf16[512,512]{1,0:T(8,128)(2,1)} %param.8) | copy-start | bytes 1572868
  336.3 54.6 %all-gather.16.cloned.1.call-start = ((), (), s32[]{:S(2)}) async-start(), calls=%async_computation.7 | async-start | bytes 2621440 | tf_op jit(solution)/shard_map/all_gather | solution.py:34
  368.2 76.4 %reduce-scatter.5.cloned.1.call-start = ((), (), s32[]{:S(2)}) async-start(), calls=%async_computation.8 | async-start | bytes 2621440 | tf_op jit(solution)/shard_map/reduce_scatter | solution.py:59
  390.9 2.2 copy-start.3
  393.1 3.1 copy-start.7
  397.5 7.1 %collective-permute-start.4 = (bf16[1,512]{1,0:T(2,128)(2,1)S(1)}, bf16[1,512]{1,0:T(2,128)(2,1)S(1)}, u32[]{:S(2)}, u32[]{:S(2)}) collective-permute-start(bf16[1,512]{1,0:T(2,128)(2,1)S(1)} %get-tuple-element.7), channel_id=1, source_target_pairs={{0,4},{4,8},{8,12},{12,16},{16,20},{20,24},{24,28},{1,5},{5,9},{9,... | collective-permute-start | bytes 3080 | tf_op jit(solution)/shard_map/ppermute | solution.py:17
  400.9 5.5 %collective-permute-start.5 = (bf16[1,512]{1,0:T(2,128)(2,1)S(1)}, bf16[1,512]{1,0:T(2,128)(2,1)S(1)}, u32[]{:S(2)}, u32[]{:S(2)}) collective-permute-start(bf16[1,512]{1,0:T(2,128)(2,1)S(1)} %get-tuple-element.8), channel_id=1, source_target_pairs={{4,0},{8,4},{12,8},{16,12},{20,16},{24,20},{28,24},{5,1},{9,5},{13... | collective-permute-start | bytes 3080 | tf_op jit(solution)/shard_map/ppermute | solution.py:18
  413.3 31.3 %copy-start = (bf16[512,512]{1,0:T(8,128)(2,1)S(1)}, bf16[512,512]{1,0:T(8,128)(2,1)}, u32[]{:S(2)}) copy-start(bf16[512,512]{1,0:T(8,128)(2,1)} %add_convert_fusion.1) | copy-start | bytes 1572868
Sparse Core Ops, SparseCore 0:
  8.9 25.2 all-gather.7
  36.4 72.7 all-gather.13
  111.4 71.2 all-gather.11
  184.7 71.3 all-gather.17
  258.1 71.2 all-gather.9
  336.4 29.7 reduce-scatter.2
  368.3 22.5 all-gather.15
  413.4 31.1 reduce-scatter.4
